TPU v7x, 32 devices: a whole 2x2x4 slice. The times are simulated.
32 devices in a mesh: ep: 32 (over z, y, x, core).
Axes of the slice: x: 2, y: 2, z: 4, core: 2. Of those that a mesh axis runs over, the one named last changes fastest.
Arguments:
- tokens: bfloat16 [32, 2048], P('ep'), may hold values from -6 to 6
- mixer_gain: float32 [2048], replicated, may hold values from 0.1 to 1.9
- query_weight: bfloat16 [2048, 2048], P(None, 'ep'), may hold values from -0.125 to 0.125
- key_weight: bfloat16 [2048, 2048], P(None, 'ep'), may hold values from -0.125 to 0.125
- value_weight: bfloat16 [2048, 2048], P(None, 'ep'), may hold values from -0.125 to 0.125
- outgate_weight: bfloat16 [2048, 2048], P(None, 'ep'), may hold values from -0.125 to 0.125
- input_weight: bfloat16 [2048, 4], replicated, may hold values from -0.125 to 0.125
- forget_weight: bfloat16 [2048, 4], replicated, may hold values from -0.125 to 0.125
- forget_bias: float32 [4], replicated, may hold values from 0 to 4
- memory_matrix: float32 [32, 4, 512, 512], P('ep'), may hold values from -0.3 to 0.3
- memory_norm: float32 [32, 4, 512], P('ep'), may hold values from -0.3 to 0.3
- memory_max: float32 [32, 4], P('ep'), may hold values from -2 to 2
- mixer_out: bfloat16 [2048, 2048], P(None, 'ep'), may hold values from -0.125 to 0.125
- expert_gain: float32 [2048], replicated, may hold values from 0.1 to 1.9
- expert_gate: bfloat16 [32, 2048, 1024], P('ep'), may hold values from -0.125 to 0.125
- expert_up: bfloat16 [32, 2048, 1024], P('ep'), may hold values from -0.125 to 0.125
- expert_down: bfloat16 [32, 1024, 2048], P('ep'), may hold values from -0.1875 to 0.1875
- route_group: int32 [32], P('ep'), may hold values from 0 to 3
- route_member: int32 [32, 2], P('ep'), may hold values from 0 to 7, as said below
- group_weight: float32 [32], P('ep'), may hold values from 0.25 to 1
- member_weight: float32 [32, 2], P('ep'), may hold values from 0.1 to 1
Outputs:
- layer_out: bfloat16 [32, 2048], P('ep')
- next_matrix: float32 [32, 4, 512, 512], P('ep')
- next_norm: float32 [32, 4, 512], P('ep')
- next_max: float32 [32, 4], P('ep')
Inputs may be any that keep to these rules, and one draw needn't show every extreme that they name: A row's 2 experts, numbered route_group * 8 + route_member, are different members of the one group that route_group names. No expert is named by more than 4 rows in all, and one expert is named by exactly 4 rows.
All inputs are finite; a program needn't handle non-finite values.
Results may differ from a plain program's by a relative error of at most 0.013.
Values may be sent and summed in bfloat16 or wider, within the bound.
No kernel may reach another device: no remote copies, remote signals or barrier semaphores. Data moves between devices by JAX's collectives and lax.ppermute only.
A program may use at most 64 MiB of HBM per device.

v0:
```python
import jax
import jax.numpy as jnp
from jax import lax
from jax.sharding import PartitionSpec as P

GROUPS = 4
CAPACITY = 4
norm_eps = 1e-06


def root_norm(values, gain):
    return values * lax.rsqrt(jnp.mean(values * values, axis=-1, keepdims=True) + norm_eps) * gain


def run_expert(slot_rows, gate_mat, up_mat, down_mat):
    gate_part = jnp.dot(slot_rows, gate_mat, preferred_element_type=jnp.float32)
    up_part = jnp.dot(slot_rows, up_mat, preferred_element_type=jnp.float32)
    hidden = (jax.nn.silu(gate_part) * up_part).astype(jnp.bfloat16)
    return jnp.dot(hidden, down_mat, preferred_element_type=jnp.float32).astype(jnp.bfloat16)


def local(
    tokens,
    mixer_gain,
    query_weight,
    key_weight,
    value_weight,
    outgate_weight,
    input_weight,
    forget_weight,
    forget_bias,
    memory_matrix,
    memory_norm,
    memory_max,
    mixer_out,
    expert_gain,
    expert_gate,
    expert_up,
    expert_down,
    route_group,
    route_member,
    group_weight,
    member_weight,
):
    devices = lax.axis_size("ep")
    local_rows = tokens.shape[0]
    width = tokens.shape[1]
    columns = query_weight.shape[1]
    heads = memory_matrix.shape[1]
    head_dim = memory_matrix.shape[2]
    members = devices * expert_gate.shape[0] // GROUPS
    stacked = jnp.concatenate([query_weight, key_weight, value_weight, outgate_weight], axis=1)
    piece = lax.all_gather(tokens, "ep", axis=0, tiled=True)
    normed = root_norm(piece.astype(jnp.float32), mixer_gain).astype(jnp.bfloat16)
    result = jnp.dot(normed, stacked, preferred_element_type=jnp.float32).astype(jnp.bfloat16)
    result = result.reshape(piece.shape[0], 4, columns)
    parts = lax.all_to_all(result, "ep", split_axis=0, concat_axis=2, tiled=True)
    resid = tokens.astype(jnp.float32)
    own_normed = root_norm(resid, mixer_gain).astype(jnp.bfloat16)
    input_pre = jnp.dot(own_normed, input_weight, preferred_element_type=jnp.float32)
    forget_pre = (
        jnp.dot(own_normed, forget_weight, preferred_element_type=jnp.float32) + forget_bias
    )
    log_forget = jax.nn.log_sigmoid(forget_pre)
    next_max = jnp.maximum(log_forget + memory_max, input_pre)
    keep = jnp.exp(log_forget + memory_max - next_max)
    admit = jnp.exp(input_pre - next_max)
    query_heads = parts[:, 0].astype(jnp.float32).reshape(local_rows, heads, head_dim)
    key_heads = parts[:, 1].astype(jnp.float32).reshape(local_rows, heads, head_dim) * head_dim ** (
        -0.5
    )
    value_heads = parts[:, 2].astype(jnp.float32).reshape(local_rows, heads, head_dim)
    carried = jnp.einsum(
        "shij,shj->shi", memory_matrix, query_heads, precision=lax.Precision.HIGHEST
    )
    score = jnp.sum(key_heads * query_heads, axis=-1)
    numer = keep[..., None] * carried + (admit * score)[..., None] * value_heads
    denom = keep * jnp.sum(memory_norm * query_heads, axis=-1) + admit * score
    head_out = numer / jnp.maximum(jnp.abs(denom), jnp.exp(-next_max))[..., None]
    gated = (
        head_out.reshape(local_rows, width) * jax.nn.sigmoid(parts[:, 3].astype(jnp.float32))
    ).astype(jnp.bfloat16)
    next_matrix = (
        keep[..., None, None] * memory_matrix
        + admit[..., None, None] * value_heads[..., :, None] * key_heads[..., None, :]
    )
    next_norm = keep[..., None] * memory_norm + admit[..., None] * key_heads
    proj_cols = jnp.dot(
        lax.all_gather(gated, "ep", axis=0, tiled=True),
        mixer_out,
        preferred_element_type=jnp.float32,
    ).astype(jnp.bfloat16)
    slot_index = jnp.arange(CAPACITY, dtype=jnp.int32)
    chosen_local = route_group[:, None] * members + route_member
    row_numbers = jnp.arange(local_rows, dtype=jnp.int32)
    local_weight = group_weight[:, None] * member_weight
    projected = lax.all_to_all(proj_cols, "ep", split_axis=0, concat_axis=1, tiled=True)
    middle = (resid + projected.astype(jnp.float32)).astype(jnp.bfloat16)
    expert_in = root_norm(middle.astype(jnp.float32), expert_gain).astype(jnp.bfloat16)
    targets = jnp.arange(devices, dtype=jnp.int32)
    hit = jnp.any(chosen_local[:, :, None] == targets[None, None, :], axis=1)
    outgoing = jnp.where(hit.T[:, :, None], expert_in[None, :, :], jnp.zeros((), jnp.bfloat16))
    present = hit.T.astype(jnp.bfloat16)
    incoming, flags = (
        lax.all_to_all(outgoing, "ep", split_axis=0, concat_axis=0, tiled=True),
        lax.all_to_all(present, "ep", split_axis=0, concat_axis=0, tiled=True),
    )
    flat_rows = incoming.reshape(devices * local_rows, width)
    live = (flags.reshape(devices * local_rows) > 0.5).astype(jnp.int32)
    position = jnp.cumsum(live) - 1
    select = ((position[None, :] == slot_index[:, None]) & (live[None, :] > 0)).astype(jnp.bfloat16)
    slot_rows = jnp.dot(select, flat_rows, preferred_element_type=jnp.float32).astype(jnp.bfloat16)
    finished = run_expert(slot_rows, expert_gate[0], expert_up[0], expert_down[0])
    back_rows = jnp.dot(select.T, finished, preferred_element_type=jnp.float32).astype(jnp.bfloat16)
    returned = lax.all_to_all(
        back_rows.reshape(devices, local_rows, width), "ep", split_axis=0, concat_axis=0, tiled=True
    )
    picked = returned[chosen_local.T, row_numbers[None, :]]
    mixture = jnp.sum(local_weight.T[:, :, None] * picked.astype(jnp.float32), axis=0)
    layer_out = (middle.astype(jnp.float32) + mixture).astype(jnp.bfloat16)
    return (layer_out, next_matrix, next_norm, next_max)


def solution(mesh):
    placed = (
        P("ep", None),
        P(),
        P(None, "ep"),
        P(None, "ep"),
        P(None, "ep"),
        P(None, "ep"),
        P(),
        P(),
        P(),
        P("ep", None, None, None),
        P("ep", None, None),
        P("ep", None),
        P(None, "ep"),
        P(),
        P("ep", None, None),
        P("ep", None, None),
        P("ep", None, None),
        P("ep"),
        P("ep", None),
        P("ep"),
        P("ep", None),
    )
    return jax.shard_map(
        local,
        mesh=mesh,
        in_specs=placed,
        out_specs=(P("ep", None), P("ep", None, None, None), P("ep", None, None), P("ep", None)),
        check_vma=False,
    )
```

profile of v0, /device:TPU:0, one launch (start us, length us, event | category | flops | bytes accessed | tf_op | source)
XLA Modules:
  0.0 155.1 jit_solution(15445792464496646408)
XLA Ops:
  0.7 44.3 %all-gather = bf16[32,1,2048]{2,1,0:T(2,128)(2,1)S(1)} all-gather(bf16[1,1,2048]{2,1,0:T(2,128)(2,1)} %bitcast.134), channel_id=1, replica_groups=mesh['ep'=32] {'ep'}, dimensions={0}, use_global_device_ids=true | all-gather | bytes 135168 | tf_op jit(solution)/shard_map/all_gather | solution.py:53
  45.1 0.3 convert_element_type.241
  45.6 1.6 %convolution_convert_fusion.2 = bf16[32,256]{1,0:T(8,128)(2,1)S(1)} fusion(bf16[2048,64]{0,1:T(8,128)(2,1)} %param.26, bf16[2048,64]{0,1:T(8,128)(2,1)} %param.25, bf16[2048,64]{0,1:T(8,128)(2,1)} %param.24, bf16[2048,64]{0,1:T(8,128)(2,1)} %param.23, f32[32,1,2048]{2,1,0:T(1,128)S(1)} %convert_element_type.241, f32[2048]{0:T(1024)} %param.22, ...), kind=kOutput, calls=%fused_computation.14 | convolution fusion | flops 37953536 | bytes 1335424 | tf_op jit(solution)/shard_map/dot_general | solution.py:55
  47.3 0.7 reshape.614
  48.0 2.5 %all-to-all-start = ((bf16[32,2,128]{2,1,0:T(2,128)(2,1)}), bf16[32,2,128]{2,1,0:T(2,128)(2,1)S(1)}, u32[]{:S(2)}, u32[]{:S(2)}) async-start(bf16[32,2,128]{2,1,0:T(2,128)(2,1)} %reshape.614), calls=%async_computation | async-start | bytes 32768 | tf_op jit(solution)/shard_map/all_to_all | solution.py:57
  50.6 0.6 multiply_reduce_fusion.4
  53.8 3.9 %all-to-all-done = bf16[32,2,128]{2,1,0:T(2,128)(2,1)S(1)} async-done(((bf16[32,2,128]{2,1,0:T(2,128)(2,1)}), bf16[32,2,128]{2,1,0:T(2,128)(2,1)S(1)}, u32[]{:S(2)}, u32[]{:S(2)}) %all-to-all-start) | async-done | bytes 16416 | tf_op jit(solution)/shard_map/all_to_all | solution.py:57
  58.0 4.1 %fusion.6 = f32[4,1,512]{2,1,0:T(1,128)S(1)} fusion(bf16[4,512,1]{1,2,0:T(2,128)(2,1)S(1)} %bitcast.137, f32[1,4,512,512]{3,2,1,0:T(8,128)} %param.30), kind=kOutput, calls=%fused_computation.7 | convolution fusion | flops 12582912 | bytes 4206592 | tf_op jit(solution)/shard_map/shij,shj->shi/dot_general | solution.py:73
  62.2 0.8 multiply_reduce_fusion.3
  63.1 38.6 %all-gather.1 = bf16[32,1,2048]{2,1,0:T(2,128)(2,1)S(1)} all-gather(bf16[1,1,2048]{2,1,0:T(2,128)(2,1)S(1)} %convert_bitcast_fusion), channel_id=1, replica_groups=mesh['ep'=32] {'ep'}, dimensions={0}, use_global_device_ids=true | all-gather | bytes 135168 | tf_op jit(solution)/shard_map/all_gather | solution.py:89
  102.0 0.6 copy.45
  102.6 2.5 %all-to-all-start.1 = ((bf16[32,1,64]{2,1,0:T(2,128)(2,1)}), bf16[32,1,64]{2,1,0:T(2,128)(2,1)S(1)}, u32[]{:S(2)}, u32[]{:S(2)}) async-start(bf16[32,1,64]{2,1,0:T(2,128)(2,1)} %copy.45), calls=%async_computation.1 | async-start | bytes 32768 | tf_op jit(solution)/shard_map/all_to_all | solution.py:97
  105.4 0.7 copy.46
  106.1 6.2 %all-to-all-done.1 = bf16[32,1,64]{2,1,0:T(2,128)(2,1)S(1)} async-done(((bf16[32,1,64]{2,1,0:T(2,128)(2,1)}), bf16[32,1,64]{2,1,0:T(2,128)(2,1)S(1)}, u32[]{:S(2)}, u32[]{:S(2)}) %all-to-all-start.1) | async-done | bytes 4128 | tf_op jit(solution)/shard_map/all_to_all | solution.py:97
  112.3 2.6 %all-to-all-start.2 = ((bf16[32,1,1]{2,1,0:T(2,128)(2,1)}), bf16[32,1,1]{2,1,0:T(2,128)(2,1)S(1)}, u32[]{:S(2)}, u32[]{:S(2)}) async-start(bf16[32,1,1]{2,1,0:T(2,128)(2,1)} %copy.46), calls=%async_computation.2 | async-start | bytes 32768 | tf_op jit(solution)/shard_map/all_to_all | solution.py:106
  115.0 0.6 multiply_reduce_fusion.1
  116.6 0.5 broadcast.318
  117.1 1.4 reduce.34
  118.5 0.7 reshape.616
  119.2 2.8 %all-to-all-done.2 = bf16[32,1,1]{2,1,0:T(2,128)(2,1)S(1)} async-done(((bf16[32,1,1]{2,1,0:T(2,128)(2,1)}), bf16[32,1,1]{2,1,0:T(2,128)(2,1)S(1)}, u32[]{:S(2)}, u32[]{:S(2)}) %all-to-all-start.2) | async-done | bytes 96 | tf_op jit(solution)/shard_map/all_to_all | solution.py:106
  122.0 3.1 %all-to-all-start.3 = ((bf16[32,2,1024]{2,1,0:T(2,128)(2,1)}), bf16[32,2,1024]{2,1,0:T(2,128)(2,1)S(1)}, u32[]{:S(2)}, u32[]{:S(2)}) async-start(bf16[32,2,1024]{2,1,0:T(2,128)(2,1)} %reshape.616), calls=%async_computation.3 | async-start | bytes 262144 | tf_op jit(solution)/shard_map/all_to_all | solution.py:105
  125.1 0.7 compare_reduce_fusion
  125.9 7.4 %all-to-all-done.3 = bf16[32,2,1024]{2,1,0:T(2,128)(2,1)S(1)} async-done(((bf16[32,2,1024]{2,1,0:T(2,128)(2,1)}), bf16[32,2,1024]{2,1,0:T(2,128)(2,1)S(1)}, u32[]{:S(2)}, u32[]{:S(2)}) %all-to-all-start.3) | async-done | bytes 131104 | tf_op jit(solution)/shard_map/all_to_all | solution.py:105
  133.6 2.8 %fusion.4 = f32[4,1024]{1,0:T(4,128)S(1)} fusion(bf16[4,2048]{1,0:T(4,128)(2,1)S(1)} %convolution_convert_fusion.1, bf16[1,2048,1024]{2,1,0:T(8,128)(2,1)} %param.35), kind=kOutput, calls=%fused_computation.5 | convolution fusion | flops 16777216 | bytes 4227072 | tf_op jit(solution)/shard_map/dot_general | solution.py:16
  136.4 4.7 %fusion.9 = bf16[4,2048]{1,0:T(4,128)(2,1)S(1)} fusion(bf16[1,1024,2048]{2,1,0:T(8,128)(2,1)} %param.37, bf16[4,2048]{1,0:T(4,128)(2,1)S(1)} %convolution_convert_fusion.1, bf16[1,2048,1024]{2,1,0:T(8,128)(2,1)} %param.36, f32[4,1024]{1,0:T(4,128)S(1)} %fusion.4), kind=kOutput, calls=%fused_computation.12 | convolution fusion | flops 33587200 | bytes 8437760 | tf_op jit(solution)/shard_map/dot_general | solution.py:19
  141.4 0.7 reduce.35
  142.0 0.7 reshape.618
  142.8 2.6 %all-to-all-start.4 = ((bf16[32,2,1024]{2,1,0:T(2,128)(2,1)}), bf16[32,2,1024]{2,1,0:T(2,128)(2,1)S(1)}, u32[]{:S(2)}, u32[]{:S(2)}) async-start(bf16[32,2,1024]{2,1,0:T(2,128)(2,1)} %reshape.618), calls=%async_computation.4 | async-start | bytes 262144 | tf_op jit(solution)/shard_map/all_to_all | solution.py:115
  145.3 4.7 %multiply_add_fusion = f32[1,4,512,512]{3,2,1,0:T(8,128)} fusion(f32[1,4,512,512]{3,2,1,0:T(8,128)} %param.30, f32[4,512]{1,0:T(4,128)S(1)} %mul.289, f32[4,512]{1,0:T(4,128)S(1)} %get-tuple-element.15, f32[4]{0:T(128)S(1)} %fusion.68), kind=kLoop, calls=%fused_computation.9 | loop fusion | flops 3145728 | bytes 8405008 | tf_op jit(solution)/shard_map/add | solution.py:84
  150.1 3.5 %all-to-all-done.4 = bf16[32,2,1024]{2,1,0:T(2,128)(2,1)S(1)} async-done(((bf16[32,2,1024]{2,1,0:T(2,128)(2,1)}), bf16[32,2,1024]{2,1,0:T(2,128)(2,1)S(1)}, u32[]{:S(2)}, u32[]{:S(2)}) %all-to-all-start.4) | async-done | bytes 131104 | tf_op jit(solution)/shard_map/all_to_all | solution.py:115
  153.7 0.6 gather_fusion
  154.5 0.6 add_convert_fusion
  (65 shorter events, 3.1 us)
Async XLA Ops:
  0.6 101.1 %copy-start = (bf16[2048,64]{0,1:T(8,128)(2,1)S(1)}, bf16[2048,64]{0,1:T(8,128)(2,1)}, u32[]{:S(2)}) copy-start(bf16[2048,64]{0,1:T(8,128)(2,1)} %param.33) | copy-start | bytes 786436
  0.6 49.9 %copy-start.1 = (bf16[1,2048]{1,0:T(2,128)(2,1)S(1)}, bf16[1,2048]{1,0:T(2,128)(2,1)}, u32[]{:S(2)}) copy-start(bf16[1,2048]{1,0:T(2,128)(2,1)} %param.21) | copy-start | bytes 12292
  0.7 52.7 %copy-start.2 = (f32[2048]{0:T(1024)S(1)}, f32[2048]{0:T(1024)}, u32[]{:S(2)}) copy-start(f32[2048]{0:T(1024)} %param.22) | copy-start | bytes 24580
  0.7 51.2 %copy-start.8 = (s32[1,2]{1,0:T(1,128)S(1)}, s32[1,2]{1,0:T(1,128)}, u32[]{:S(2)}) copy-start(s32[1,2]{1,0:T(1,128)} %param.39) | copy-start | bytes 28
  0.7 52.7 %copy-start.9 = (f32[1,4]{1,0:T(1,128)S(1)}, f32[1,4]{1,0:T(1,128)}, u32[]{:S(2)}) copy-start(f32[1,4]{1,0:T(1,128)} %param.32) | copy-start | bytes 52
  0.7 52.7 %copy-start.10 = (f32[4]{0:T(128)S(1)}, f32[4]{0:T(128)}, u32[]{:S(2)}) copy-start(f32[4]{0:T(128)} %param.29) | copy-start | bytes 52
  0.7 52.7 %copy-start.6 = (bf16[2048,4]{0,1:T(4,128)(2,1)S(1)}, bf16[2048,4]{0,1:T(4,128)(2,1)}, u32[]{:S(2)}) copy-start(bf16[2048,4]{0,1:T(4,128)(2,1)} %param.28) | copy-start | bytes 49156
  0.7 52.9 %copy-start.7 = (bf16[2048,4]{0,1:T(4,128)(2,1)S(1)}, bf16[2048,4]{0,1:T(4,128)(2,1)}, u32[]{:S(2)}) copy-start(bf16[2048,4]{0,1:T(4,128)(2,1)} %param.27) | copy-start | bytes 49156
  0.7 53.0 %copy-start.11 = (f32[1,2]{1,0:T(1,128)S(1)}, f32[1,2]{1,0:T(1,128)}, u32[]{:S(2)}) copy-start(f32[1,2]{1,0:T(1,128)} %param.41) | copy-start | bytes 28
  45.5 16.6 %copy-start.3 = (f32[1,4,512]{2,1,0:T(4,128)S(1)}, f32[1,4,512]{2,1,0:T(4,128)}, u32[]{:S(2)}) copy-start(f32[1,4,512]{2,1,0:T(4,128)} %param.31) | copy-start | bytes 24580
  45.5 70.8 %copy-start.4 = (f32[2048]{0:T(1024)S(1)}, f32[2048]{0:T(1024)}, u32[]{:S(2)}) copy-start(f32[2048]{0:T(1024)} %param.34) | copy-start | bytes 24580
  48.0 9.7 %all-to-all-start = ((bf16[32,2,128]{2,1,0:T(2,128)(2,1)}), bf16[32,2,128]{2,1,0:T(2,128)(2,1)S(1)}, u32[]{:S(2)}, u32[]{:S(2)}) async-start(bf16[32,2,128]{2,1,0:T(2,128)(2,1)} %reshape.614), calls=%async_computation | async-start | bytes 32768 | tf_op jit(solution)/shard_map/all_to_all | solution.py:57
  53.7 82.7 %copy-start.5 = (f32[1,4]{1,0:T(1,128)}, f32[1,4]{1,0:T(1,128)S(1)}, u32[]{:S(2)}) copy-start(f32[1,4]{1,0:T(1,128)S(1)} %get-tuple-element.11) | copy-start | bytes 52
  102.6 9.7 %all-to-all-start.1 = ((bf16[32,1,64]{2,1,0:T(2,128)(2,1)}), bf16[32,1,64]{2,1,0:T(2,128)(2,1)S(1)}, u32[]{:S(2)}, u32[]{:S(2)}) async-start(bf16[32,1,64]{2,1,0:T(2,128)(2,1)} %copy.45), calls=%async_computation.1 | async-start | bytes 32768 | tf_op jit(solution)/shard_map/all_to_all | solution.py:97
  112.3 9.7 %all-to-all-start.2 = ((bf16[32,1,1]{2,1,0:T(2,128)(2,1)}), bf16[32,1,1]{2,1,0:T(2,128)(2,1)S(1)}, u32[]{:S(2)}, u32[]{:S(2)}) async-start(bf16[32,1,1]{2,1,0:T(2,128)(2,1)} %copy.46), calls=%async_computation.2 | async-start | bytes 32768 | tf_op jit(solution)/shard_map/all_to_all | solution.py:106
  122.0 11.3 %all-to-all-start.3 = ((bf16[32,2,1024]{2,1,0:T(2,128)(2,1)}), bf16[32,2,1024]{2,1,0:T(2,128)(2,1)S(1)}, u32[]{:S(2)}, u32[]{:S(2)}) async-start(bf16[32,2,1024]{2,1,0:T(2,128)(2,1)} %reshape.616), calls=%async_computation.3 | async-start | bytes 262144 | tf_op jit(solution)/shard_map/all_to_all | solution.py:105
  142.8 10.8 %all-to-all-start.4 = ((bf16[32,2,1024]{2,1,0:T(2,128)(2,1)}), bf16[32,2,1024]{2,1,0:T(2,128)(2,1)S(1)}, u32[]{:S(2)}, u32[]{:S(2)}) async-start(bf16[32,2,1024]{2,1,0:T(2,128)(2,1)} %reshape.618), calls=%async_computation.4 | async-start | bytes 262144 | tf_op jit(solution)/shard_map/all_to_all | solution.py:115
where the time goes:
time: 156 us; the launch traced here: 155 us
  blocking collectives  83 us (53%)
  waiting for transfers between devices  23.7 us (15%)
  matrix products  14.3 us (9%)
  starting transfers between devices  13.3 us (9%)
  other arithmetic  11.7 us (8%)
  local copies, waits for them, and re-layouts  5.47 us (4%)
  between operations  3.69 us (2%)
    all_gather x1, blocking collectives, local(): piece = lax.all_gather(tokens, 'ep', axis=0, tiled=True)  44.3 us
    all_gather x1, blocking collectives, local(): lax.all_gather(gated, 'ep', axis=0, tiled=True)  38.6 us
    all_to_all x1, waiting for transfers between devices, local(): lax.all_to_all(outgoing, 'ep', split_axis=0, concat_axis=0, tiled=True)  7.35 us
    all_to_all x1, waiting for transfers between devices, local(): lax.all_to_all(proj_cols, 'ep', split_axis=0, concat_axis=1, tiled=True)  6.21 us
    add x1, other arithmetic, local(): keep[..., None, None] * memory_matrix  4.74 us
    dot_general x1, matrix products, run_expert(): jnp.dot(hidden, down_mat, preferred_element_type=jnp.float32)  4.68 us
    dot_general x1, matrix products, local(): jnp.einsum('shij,shj->shi', memory_matrix, query_heads, precision=lax.Pre...  4.15 us
    all_to_all x1, waiting for transfers between devices, local(): lax.all_to_all(result, 'ep', split_axis=0, concat_axis=2, tiled=True)  3.87 us
  transfers between devices with their start and end apart: 5, of which 5 were waited for; matrix products, arithmetic and copies ran while one was open for 7% of the time, Pallas kernels for 0%

commit v1 on v0

--- a/solution.py
+++ b/solution.py
@@ -2,6 +2,7 @@
 import jax.numpy as jnp
 from jax import lax
 from jax.sharding import PartitionSpec as P
+from jax.lax import all_to_all, psum
 
 GROUPS = 4
 CAPACITY = 4
@@ -94,7 +95,15 @@
     chosen_local = route_group[:, None] * members + route_member
     row_numbers = jnp.arange(local_rows, dtype=jnp.int32)
     local_weight = group_weight[:, None] * member_weight
-    projected = lax.all_to_all(proj_cols, "ep", split_axis=0, concat_axis=1, tiled=True)
+    projected = jnp.concatenate(
+        all_to_all(
+            jnp.stack(jnp.split(proj_cols, psum(1, axis_name="ep"), axis=0)),
+            split_axis=0,
+            axis_name="ep",
+            concat_axis=0,
+        ),
+        axis=1,
+    )
     middle = (resid + projected.astype(jnp.float32)).astype(jnp.bfloat16)
     expert_in = root_norm(middle.astype(jnp.float32), expert_gain).astype(jnp.bfloat16)
     targets = jnp.arange(devices, dtype=jnp.int32)

time: 156 us -> 171 us (1.096)
  local copies, waits for them, and re-layouts: 5.47 us -> 21.3 us
    unnamed x32 -> x63, local copies, waits for them, and re-layouts: 2.59 us -> 18.5 us
where the time goes in v1:
time: 171 us
  blocking collectives  83 us (49%)
  waiting for transfers between devices  23.7 us (14%)
  local copies, waits for them, and re-layouts  21.3 us (12%)
  matrix products  14.2 us (8%)
  starting transfers between devices  13.3 us (8%)
  other arithmetic  11.7 us (7%)
  between operations  3.71 us (2%)
    all_gather x1, blocking collectives, local(): piece = lax.all_gather(tokens, 'ep', axis=0, tiled=True)  44.3 us
    all_gather x1, blocking collectives, local(): lax.all_gather(gated, 'ep', axis=0, tiled=True)  38.6 us
    unnamed x63, local copies, waits for them, and re-layouts  18.5 us
    all_to_all x1, waiting for transfers between devices, local(): lax.all_to_all(outgoing, 'ep', split_axis=0, concat_axis=0, tiled=True)  7.35 us
    all_to_all x1, waiting for transfers between devices, local(): all_to_all(jnp.stack(jnp.split(proj_cols, psum(1, axis_name='ep'), axis=0...  6.21 us
    add x1, other arithmetic, local(): keep[..., None, None] * memory_matrix  4.74 us
    dot_general x1, matrix products, run_expert(): jnp.dot(hidden, down_mat, preferred_element_type=jnp.float32)  4.68 us
    dot_general x1, matrix products, local(): jnp.einsum('shij,shj->shi', memory_matrix, query_heads, precision=lax.Pre...  4.15 us
  transfers between devices with their start and end apart: 5, of which 5 were waited for; matrix products, arithmetic and copies ran while one was open for 7% of the time, Pallas kernels for 0%

profile of v1, /device:TPU:0, one launch (start us, length us, event | category | flops | bytes accessed | tf_op | source)
XLA Modules:
  0.0 170.9 jit_solution(8038498227252386467)
XLA Ops:
  0.7 44.3 %all-gather = bf16[32,1,2048]{2,1,0:T(2,128)(2,1)S(1)} all-gather(bf16[1,1,2048]{2,1,0:T(2,128)(2,1)} %bitcast.260), channel_id=1, replica_groups=mesh['ep'=32] {'ep'}, dimensions={0}, use_global_device_ids=true | all-gather | bytes 135168 | tf_op jit(solution)/shard_map/all_gather | solution.py:54
  45.6 1.6 convolution_convert_fusion.2
  47.3 0.7 reshape.609
  48.0 2.5 %all-to-all-start = ((bf16[32,2,128]{2,1,0:T(2,128)(2,1)}), bf16[32,2,128]{2,1,0:T(2,128)(2,1)S(1)}, u32[]{:S(2)}, u32[]{:S(2)}) async-start(bf16[32,2,128]{2,1,0:T(2,128)(2,1)} %reshape.609), calls=%async_computation | async-start | bytes 32768 | tf_op jit(solution)/shard_map/all_to_all | solution.py:58
  50.6 0.6 multiply_reduce_fusion.4
  53.8 3.9 %all-to-all-done = bf16[32,2,128]{2,1,0:T(2,128)(2,1)S(1)} async-done(((bf16[32,2,128]{2,1,0:T(2,128)(2,1)}), bf16[32,2,128]{2,1,0:T(2,128)(2,1)S(1)}, u32[]{:S(2)}, u32[]{:S(2)}) %all-to-all-start) | async-done | bytes 16416 | tf_op jit(solution)/shard_map/all_to_all | solution.py:58
  58.0 4.1 %fusion.6 = f32[4,1,512]{2,1,0:T(1,128)S(1)} fusion(bf16[4,512,1]{1,2,0:T(2,128)(2,1)S(1)} %bitcast.263, f32[1,4,512,512]{3,2,1,0:T(8,128)} %param.30), kind=kOutput, calls=%fused_computation.7 | convolution fusion | flops 12582912 | bytes 4206592 | tf_op jit(solution)/shard_map/shij,shj->shi/dot_general | solution.py:74
  62.2 0.8 multiply_reduce_fusion.3
  63.1 38.6 %all-gather.1 = bf16[32,1,2048]{2,1,0:T(2,128)(2,1)S(1)} all-gather(bf16[1,1,2048]{2,1,0:T(2,128)(2,1)S(1)} %convert_bitcast_fusion), channel_id=1, replica_groups=mesh['ep'=32] {'ep'}, dimensions={0}, use_global_device_ids=true | all-gather | bytes 135168 | tf_op jit(solution)/shard_map/all_gather | solution.py:90
  102.5 0.5 constant_dynamic-update-slice_fusion.30
  103.0 0.5 constant_dynamic-update-slice_fusion.29
  103.5 0.5 constant_dynamic-update-slice_fusion.28
  118.5 2.5 %all-to-all-start.1 = ((bf16[32,1,64]{2,1,0:T(2,128)(2,1)}), bf16[32,1,64]{2,1,0:T(2,128)(2,1)S(1)}, u32[]{:S(2)}, u32[]{:S(2)}) async-start(bf16[32,1,64]{2,1,0:T(2,128)(2,1)} %constant_dynamic-update-slice_fusion), calls=%async_computation.1 | async-start | bytes 32768 | tf_op jit(solution)/shard_map/all_to_all | solution.py:99
  121.2 0.7 copy.43
  121.9 6.2 %all-to-all-done.1 = bf16[32,1,64]{2,1,0:T(2,128)(2,1)S(1)} async-done(((bf16[32,1,64]{2,1,0:T(2,128)(2,1)}), bf16[32,1,64]{2,1,0:T(2,128)(2,1)S(1)}, u32[]{:S(2)}, u32[]{:S(2)}) %all-to-all-start.1) | async-done | bytes 4128 | tf_op jit(solution)/shard_map/all_to_all | solution.py:99
  128.1 2.6 %all-to-all-start.2 = ((bf16[32,1,1]{2,1,0:T(2,128)(2,1)}), bf16[32,1,1]{2,1,0:T(2,128)(2,1)S(1)}, u32[]{:S(2)}, u32[]{:S(2)}) async-start(bf16[32,1,1]{2,1,0:T(2,128)(2,1)} %copy.43), calls=%async_computation.2 | async-start | bytes 32768 | tf_op jit(solution)/shard_map/all_to_all | solution.py:115
  130.8 0.6 multiply_reduce_fusion.1
  133.0 1.4 reduce.34
  134.4 0.7 reshape.611
  135.1 2.8 %all-to-all-done.2 = bf16[32,1,1]{2,1,0:T(2,128)(2,1)S(1)} async-done(((bf16[32,1,1]{2,1,0:T(2,128)(2,1)}), bf16[32,1,1]{2,1,0:T(2,128)(2,1)S(1)}, u32[]{:S(2)}, u32[]{:S(2)}) %all-to-all-start.2) | async-done | bytes 96 | tf_op jit(solution)/shard_map/all_to_all | solution.py:115
  137.9 3.1 %all-to-all-start.3 = ((bf16[32,2,1024]{2,1,0:T(2,128)(2,1)}), bf16[32,2,1024]{2,1,0:T(2,128)(2,1)S(1)}, u32[]{:S(2)}, u32[]{:S(2)}) async-start(bf16[32,2,1024]{2,1,0:T(2,128)(2,1)} %reshape.611), calls=%async_computation.3 | async-start | bytes 262144 | tf_op jit(solution)/shard_map/all_to_all | solution.py:114
  140.9 0.7 compare_reduce_fusion
  141.8 7.4 %all-to-all-done.3 = bf16[32,2,1024]{2,1,0:T(2,128)(2,1)S(1)} async-done(((bf16[32,2,1024]{2,1,0:T(2,128)(2,1)}), bf16[32,2,1024]{2,1,0:T(2,128)(2,1)S(1)}, u32[]{:S(2)}, u32[]{:S(2)}) %all-to-all-start.3) | async-done | bytes 131104 | tf_op jit(solution)/shard_map/all_to_all | solution.py:114
  149.4 2.8 %fusion.4 = f32[4,1024]{1,0:T(4,128)S(1)} fusion(bf16[4,2048]{1,0:T(4,128)(2,1)S(1)} %convolution_convert_fusion.1, bf16[1,2048,1024]{2,1,0:T(8,128)(2,1)} %param.35), kind=kOutput, calls=%fused_computation.5 | convolution fusion | flops 16777216 | bytes 4227072 | tf_op jit(solution)/shard_map/dot_general | solution.py:17
  152.3 4.7 %fusion.9 = bf16[4,2048]{1,0:T(4,128)(2,1)S(1)} fusion(bf16[1,1024,2048]{2,1,0:T(8,128)(2,1)} %param.37, bf16[4,2048]{1,0:T(4,128)(2,1)S(1)} %convolution_convert_fusion.1, bf16[1,2048,1024]{2,1,0:T(8,128)(2,1)} %param.36, f32[4,1024]{1,0:T(4,128)S(1)} %fusion.4), kind=kOutput, calls=%fused_computation.12 | convolution fusion | flops 33587200 | bytes 8437760 | tf_op jit(solution)/shard_map/dot_general | solution.py:20
  157.2 0.7 reduce.35
  157.9 0.7 reshape.613
  158.6 2.6 %all-to-all-start.4 = ((bf16[32,2,1024]{2,1,0:T(2,128)(2,1)}), bf16[32,2,1024]{2,1,0:T(2,128)(2,1)S(1)}, u32[]{:S(2)}, u32[]{:S(2)}) async-start(bf16[32,2,1024]{2,1,0:T(2,128)(2,1)} %reshape.613), calls=%async_computation.4 | async-start | bytes 262144 | tf_op jit(solution)/shard_map/all_to_all | solution.py:124
  161.2 4.7 %multiply_add_fusion = f32[1,4,512,512]{3,2,1,0:T(8,128)} fusion(f32[1,4,512,512]{3,2,1,0:T(8,128)} %param.30, f32[4,512]{1,0:T(4,128)S(1)} %mul.289, f32[4,512]{1,0:T(4,128)S(1)} %get-tuple-element.15, f32[4]{0:T(128)S(1)} %fusion.67), kind=kLoop, calls=%fused_computation.9 | loop fusion | flops 3145728 | bytes 8405008 | tf_op jit(solution)/shard_map/add | solution.py:85
  165.9 3.5 %all-to-all-done.4 = bf16[32,2,1024]{2,1,0:T(2,128)(2,1)S(1)} async-done(((bf16[32,2,1024]{2,1,0:T(2,128)(2,1)}), bf16[32,2,1024]{2,1,0:T(2,128)(2,1)S(1)}, u32[]{:S(2)}, u32[]{:S(2)}) %all-to-all-start.4) | async-done | bytes 131104 | tf_op jit(solution)/shard_map/all_to_all | solution.py:124
  169.6 0.6 gather_fusion
  170.3 0.6 add_convert_fusion
  (96 shorter events, 18.8 us)
Async XLA Ops:
  0.6 101.1 %copy-start = (bf16[2048,64]{0,1:T(8,128)(2,1)S(1)}, bf16[2048,64]{0,1:T(8,128)(2,1)}, u32[]{:S(2)}) copy-start(bf16[2048,64]{0,1:T(8,128)(2,1)} %param.33) | copy-start | bytes 786436
  0.6 49.9 %copy-start.1 = (bf16[1,2048]{1,0:T(2,128)(2,1)S(1)}, bf16[1,2048]{1,0:T(2,128)(2,1)}, u32[]{:S(2)}) copy-start(bf16[1,2048]{1,0:T(2,128)(2,1)} %param.21) | copy-start | bytes 12292
  0.7 52.7 %copy-start.2 = (f32[2048]{0:T(1024)S(1)}, f32[2048]{0:T(1024)}, u32[]{:S(2)}) copy-start(f32[2048]{0:T(1024)} %param.22) | copy-start | bytes 24580
  0.7 51.2 %copy-start.8 = (s32[1,2]{1,0:T(1,128)S(1)}, s32[1,2]{1,0:T(1,128)}, u32[]{:S(2)}) copy-start(s32[1,2]{1,0:T(1,128)} %param.39) | copy-start | bytes 28
  0.7 52.7 %copy-start.9 = (f32[1,4]{1,0:T(1,128)S(1)}, f32[1,4]{1,0:T(1,128)}, u32[]{:S(2)}) copy-start(f32[1,4]{1,0:T(1,128)} %param.32) | copy-start | bytes 52
  0.7 52.7 %copy-start.10 = (f32[4]{0:T(128)S(1)}, f32[4]{0:T(128)}, u32[]{:S(2)}) copy-start(f32[4]{0:T(128)} %param.29) | copy-start | bytes 52
  0.7 52.7 %copy-start.6 = (bf16[2048,4]{0,1:T(4,128)(2,1)S(1)}, bf16[2048,4]{0,1:T(4,128)(2,1)}, u32[]{:S(2)}) copy-start(bf16[2048,4]{0,1:T(4,128)(2,1)} %param.28) | copy-start | bytes 49156
  0.7 52.9 %copy-start.7 = (bf16[2048,4]{0,1:T(4,128)(2,1)S(1)}, bf16[2048,4]{0,1:T(4,128)(2,1)}, u32[]{:S(2)}) copy-start(bf16[2048,4]{0,1:T(4,128)(2,1)} %param.27) | copy-start | bytes 49156
  0.7 53.0 %copy-start.11 = (f32[1,2]{1,0:T(1,128)S(1)}, f32[1,2]{1,0:T(1,128)}, u32[]{:S(2)}) copy-start(f32[1,2]{1,0:T(1,128)} %param.41) | copy-start | bytes 28
  45.5 16.6 %copy-start.3 = (f32[1,4,512]{2,1,0:T(4,128)S(1)}, f32[1,4,512]{2,1,0:T(4,128)}, u32[]{:S(2)}) copy-start(f32[1,4,512]{2,1,0:T(4,128)} %param.31) | copy-start | bytes 24580
  45.5 86.6 %copy-start.4 = (f32[2048]{0:T(1024)S(1)}, f32[2048]{0:T(1024)}, u32[]{:S(2)}) copy-start(f32[2048]{0:T(1024)} %param.34) | copy-start | bytes 24580
  48.0 9.7 %all-to-all-start = ((bf16[32,2,128]{2,1,0:T(2,128)(2,1)}), bf16[32,2,128]{2,1,0:T(2,128)(2,1)S(1)}, u32[]{:S(2)}, u32[]{:S(2)}) async-start(bf16[32,2,128]{2,1,0:T(2,128)(2,1)} %reshape.609), calls=%async_computation | async-start | bytes 32768 | tf_op jit(solution)/shard_map/all_to_all | solution.py:58
  53.7 98.6 %copy-start.5 = (f32[1,4]{1,0:T(1,128)}, f32[1,4]{1,0:T(1,128)S(1)}, u32[]{:S(2)}) copy-start(f32[1,4]{1,0:T(1,128)S(1)} %get-tuple-element.11) | copy-start | bytes 52
  118.5 9.7 %all-to-all-start.1 = ((bf16[32,1,64]{2,1,0:T(2,128)(2,1)}), bf16[32,1,64]{2,1,0:T(2,128)(2,1)S(1)}, u32[]{:S(2)}, u32[]{:S(2)}) async-start(bf16[32,1,64]{2,1,0:T(2,128)(2,1)} %constant_dynamic-update-slice_fusion), calls=%async_computation.1 | async-start | bytes 32768 | tf_op jit(solution)/shard_map/all_to_all | solution.py:99
  128.1 9.7 %all-to-all-start.2 = ((bf16[32,1,1]{2,1,0:T(2,128)(2,1)}), bf16[32,1,1]{2,1,0:T(2,128)(2,1)S(1)}, u32[]{:S(2)}, u32[]{:S(2)}) async-start(bf16[32,1,1]{2,1,0:T(2,128)(2,1)} %copy.43), calls=%async_computation.2 | async-start | bytes 32768 | tf_op jit(solution)/shard_map/all_to_all | solution.py:115
  137.9 11.3 %all-to-all-start.3 = ((bf16[32,2,1024]{2,1,0:T(2,128)(2,1)}), bf16[32,2,1024]{2,1,0:T(2,128)(2,1)S(1)}, u32[]{:S(2)}, u32[]{:S(2)}) async-start(bf16[32,2,1024]{2,1,0:T(2,128)(2,1)} %reshape.611), calls=%async_computation.3 | async-start | bytes 262144 | tf_op jit(solution)/shard_map/all_to_all | solution.py:114
  158.6 10.8 %all-to-all-start.4 = ((bf16[32,2,1024]{2,1,0:T(2,128)(2,1)}), bf16[32,2,1024]{2,1,0:T(2,128)(2,1)S(1)}, u32[]{:S(2)}, u32[]{:S(2)}) async-start(bf16[32,2,1024]{2,1,0:T(2,128)(2,1)} %reshape.613), calls=%async_computation.4 | async-start | bytes 262144 | tf_op jit(solution)/shard_map/all_to_all | solution.py:124
